TPU v7x, 32 devices: a whole 2x2x4 slice. The times are simulated.
32 devices in a mesh: sp: 8 (over z, y), tp: 4 (over x, core).
Axes of the slice: x: 2, y: 2, z: 4, core: 2. Of those that a mesh axis runs over, the one named last changes fastest.
Arguments:
- prompt_input: bfloat16 [2304, 2048], P('sp'), may hold values from -6 to 6
- next_input: bfloat16 [2048], replicated, may hold values from -6 to 6
- norm_gain: float32 [2048], replicated, may hold values from 0.1 to 1.9
- w_key: bfloat16 [2048, 1024], P(None, 'tp'), may hold values from -0.125 to 0.125
- w_value: bfloat16 [2048, 1024], P(None, 'tp'), may hold values from -0.125 to 0.125
- w_query: bfloat16 [2048, 1024], P(None, 'tp'), may hold values from -0.125 to 0.125
- key_offset: float32 [2304, 8], P('sp', 'tp'), may hold values from -10 to 0, as said below
Outputs:
- key_cache: bfloat16 [8, 8, 36, 1024], P('sp', None, None, 'tp')
- value_cache: bfloat16 [8, 8, 36, 1024], P('sp', None, None, 'tp')
- reading: bfloat16 [1024], replicated
Inputs may be any that keep to these rules, and one draw needn't show every extreme that they name: `key_offset`: finite log-odds offsets, one per key and head.
All inputs are finite; a program needn't handle non-finite values.
Results may differ from a plain program's by a relative error of at most 0.011.
Values may be sent and summed in bfloat16 or wider, within the bound.
A program may use at most 64 MiB of HBM per device.

v0:
```python
import jax
import jax.numpy as jnp
from jax import lax
from jax.sharding import PartitionSpec as P

HEAD_DIM = 128


def norm_rows(row_block, gain_vec):
    wide_rows = row_block.astype(jnp.float32)
    inv_rms = lax.rsqrt(jnp.mean(wide_rows * wide_rows, axis=-1, keepdims=True) + 1e-06)
    return (wide_rows * inv_rms * gain_vec).astype(jnp.bfloat16)


def shards(prompt_input, next_input, norm_gain, w_key, w_value, w_query, key_offset):
    span_len = prompt_input.shape[0]
    head_width = w_key.shape[1]
    heads_here = head_width // HEAD_DIM
    score_scale = HEAD_DIM ** (-0.5)
    slots = lax.axis_size("sp")
    sub_len = span_len // slots
    normed = norm_rows(prompt_input, norm_gain)
    key_rows = jnp.dot(normed, w_key, preferred_element_type=jnp.float32).astype(jnp.bfloat16)
    value_rows = jnp.dot(normed, w_value, preferred_element_type=jnp.float32).astype(jnp.bfloat16)
    outgoing = jnp.stack([key_rows, value_rows]).reshape(2, slots, 1, sub_len, head_width)
    arrived = lax.all_to_all(outgoing, "sp", split_axis=1, concat_axis=2, tiled=True)
    key_cache = arrived[0]
    value_cache = arrived[1]
    new_query = jnp.dot(
        norm_rows(next_input[None, :], norm_gain), w_query, preferred_element_type=jnp.float32
    )
    new_query = new_query.astype(jnp.bfloat16).reshape(heads_here, HEAD_DIM)
    key_heads = key_rows.reshape(span_len, heads_here, HEAD_DIM)
    value_heads = value_rows.reshape(span_len, heads_here, HEAD_DIM)
    logits = (
        jnp.einsum("hd,shd->sh", new_query, key_heads, preferred_element_type=jnp.float32)
        * score_scale
        + key_offset
    )
    log_breaks = jax.nn.log_sigmoid(-logits)
    inner_sum = lax.cumsum(log_breaks, axis=0, reverse=True) - log_breaks
    block_totals = jnp.sum(log_breaks, axis=0)
    every_total = lax.all_gather(block_totals[None], "sp", axis=0, tiled=True)
    block_ids = lax.broadcasted_iota(jnp.int32, every_total.shape, 0)
    carried = jnp.sum(jnp.where(block_ids > lax.axis_index("sp"), every_total, 0.0), axis=0)
    weights = jnp.exp(jax.nn.log_sigmoid(logits) + inner_sum + carried[None, :])
    partial_value = jnp.einsum("sh,shd->hd", weights, value_heads.astype(jnp.float32))
    summed = lax.psum(partial_value, "sp")
    own_read = summed.reshape(head_width).astype(jnp.bfloat16)
    reading = lax.all_gather(own_read, "tp", axis=0, tiled=True)
    return (key_cache, value_cache, reading)


def solution(mesh):
    placed = (P("sp", None), P(), P(), P(None, "tp"), P(None, "tp"), P(None, "tp"), P("sp", "tp"))
    return jax.shard_map(
        shards,
        mesh=mesh,
        in_specs=placed,
        out_specs=(P("sp", None, None, "tp"), P("sp", None, None, "tp"), P()),
        check_vma=False,
    )
```

profile of v0, /device:TPU:0, one launch (start us, length us, event | category | flops | bytes accessed | tf_op | source)
XLA Modules:
  0.0 65.4 jit_solution(9334492287471043287)
XLA Ops:
  0.7 1.7 %fusion = f32[288]{0:T(512)S(1)} fusion(bf16[288,2048]{1,0:T(8,128)(2,1)} %param.7), kind=kLoop, calls=%fused_computation.2 | loop fusion | flops 1769184 | bytes 1180800 | tf_op jit(solution)/shard_map/reduce_sum | solution.py:11
  2.4 0.2 copy-done.1
  2.6 1.3 %convolution_convert_fusion = bf16[288,256]{1,0:T(8,128)(2,1)S(1)} fusion(bf16[2048,256]{1,0:T(8,128)(2,1)S(1)} %copy-done, bf16[288,2048]{1,0:T(8,128)(2,1)S(1)} %copy-done.1, f32[2048]{0:T(1024)} %param.9, f32[288]{0:T(512)S(1)} %add_rsqrt_fusion), kind=kOutput, calls=%fused_computation.5 | convolution fusion | flops 304422912 | bytes 2385024 | tf_op jit(solution)/shard_map/dot_general | solution.py:24
  3.9 0.5 convolution_convert_fusion.1
  4.6 1.0 %copy.17 = bf16[2,8,1,36,256]{4,0,3,2,1:T(2,128)(2,1)} copy(bf16[2,8,1,36,256]{4,3,1,2,0:T(8,128)(2,1)S(1)} %pad_maximum_fusion) | data formatting | bytes 589824 | tf_op jit(solution)/shard_map/stack | solution.py:25
  5.6 7.3 %all-to-all-start = ((bf16[2,8,1,36,256]{4,0,3,2,1:T(2,128)(2,1)}), bf16[2,8,1,36,256]{4,0,3,2,1:T(2,128)(2,1)S(1)}, u32[]{:S(2)}, u32[]{:S(2)}) async-start(bf16[2,8,1,36,256]{4,0,3,2,1:T(2,128)(2,1)} %copy.17), calls=%async_computation | async-start | bytes 589824 | tf_op jit(solution)/shard_map/all_to_all | solution.py:26
  13.0 0.6 fusion.11
  14.3 0.2 fusion.21
  14.5 0.1 fusion.8
  14.7 0.6 dynamic-slice
  16.0 0.1 fusion.19
  16.1 0.1 negate_dynamic-update-slice_fusion
  16.2 21.8 %all-reduce.1 = f32[16]{0:T(128)S(1)} all-reduce(f32[16]{0:T(128)S(1)} %negate_dynamic-update-slice_fusion), channel_id=2, replica_groups=mesh['sp'=8,'tp'=4] {'sp'}, use_global_device_ids=true, to_apply=%add.1 | all-reduce | flops 16 | bytes 128
  38.1 2.5 %reduce-window.6 = f32[2,3,128]{2,1,0:T(4,128)S(1)} reduce-window(f32[2,3,128]{2,1,0:T(4,128)S(1)} %reshape.81, f32[]{:T(128)} %constant.20.clone.1), window={size=1x1x128 pad=0_0x0_0x0_127}, to_apply=%region_2.3 | reduce-window | flops 97536 | bytes 6148 | tf_op jit(solution)/shard_map/reduce-window
  40.6 0.1 slice_reduce_fusion
  40.7 0.2 reduce-window.9
  41.1 0.1 select_reduce_fusion
  41.2 0.1 exponential_bitcast_fusion
  41.3 0.1 fusion.5
  41.4 17.1 %psum.7 = bf16[2,128]{1,0:T(2,128)(2,1)S(1)} all-reduce(f32[2,128]{1,0:T(2,128)S(1)} %bitcast.64), channel_id=1, replica_groups=mesh['sp'=8,'tp'=4] {'sp'}, use_global_device_ids=true, to_apply=%region_6.7 | all-reduce | flops 256 | bytes 1536 | tf_op jit(solution)/shard_map/psum | solution.py:48
  58.6 5.1 %all-gather.1 = bf16[4,1,256]{2,1,0:T(2,128)(2,1)S(1)} all-gather(bf16[1,1,256]{2,1,0:T(2,128)(2,1)S(1)} %reshape.88), channel_id=1, replica_groups=mesh['sp'=8,'tp'=4] {'tp'}, dimensions={0}, use_global_device_ids=true | all-gather | bytes 2560 | tf_op jit(solution)/shard_map/all_gather | solution.py:50
  63.6 0.6 copy.31
  64.2 0.4 fusion.20
  64.6 0.8 %copy_bitcast_fusion = (bf16[1,8,36,256]{3,1,2,0:T(8,128)(2,1)}, bf16[1,8,36,256]{3,1,2,0:T(8,128)(2,1)}) fusion(bf16[1,8,1,36,256]{4,0,3,2,1:T(2,128)(2,1)S(1)} %get-tuple-element.11, bf16[1,8,1,36,256]{4,0,3,2,1:T(2,128)(2,1)S(1)} %get-tuple-element.12), kind=kLoop, calls=%fused_computation.14 | loop fusion | bytes 589824 | tf_op jit(solution)/shard_map/squeeze | solution.py:28
  (34 shorter events, 0.5 us)
Async XLA Ops:
  0.6 1.8 %copy-start = (bf16[2048,256]{1,0:T(8,128)(2,1)S(1)}, bf16[2048,256]{1,0:T(8,128)(2,1)}, u32[]{:S(2)}) copy-start(bf16[2048,256]{1,0:T(8,128)(2,1)} %param.11) | copy-start | bytes 3145732
  0.6 1.9 %copy-start.1 = (bf16[288,2048]{1,0:T(8,128)(2,1)S(1)}, bf16[288,2048]{1,0:T(8,128)(2,1)}, u32[]{:S(2)}) copy-start(bf16[288,2048]{1,0:T(8,128)(2,1)} %param.7) | copy-start | bytes 3538948
  2.6 1.3 %copy-start.5 = (f32[2048]{0:T(1024)S(1)}, f32[2048]{0:T(1024)}, u32[]{:S(2)}) copy-start(f32[2048]{0:T(1024)} %param.9) | copy-start | bytes 24580
  2.6 1.3 %copy-start.6 = (bf16[2048,256]{1,0:T(8,128)(2,1)S(1)}, bf16[2048,256]{1,0:T(8,128)(2,1)}, u32[]{:S(2)}) copy-start(bf16[2048,256]{1,0:T(8,128)(2,1)} %param.10) | copy-start | bytes 3145732
  4.5 8.5 %copy-start.3 = (bf16[2048]{0:T(1024)(128)(2,1)S(1)}, bf16[2048]{0:T(1024)(128)(2,1)}, u32[]{:S(2)}) copy-start(bf16[2048]{0:T(1024)(128)(2,1)} %param.8) | copy-start | bytes 12292
  4.5 9.8 %copy-start.2 = (bf16[2048,256]{1,0:T(8,128)(2,1)S(1)}, bf16[2048,256]{1,0:T(8,128)(2,1)}, u32[]{:S(2)}) copy-start(bf16[2048,256]{1,0:T(8,128)(2,1)} %param.12) | copy-start | bytes 3145732
  4.6 10.1 %copy-start.7 = (u32[32]{0:T(128)S(1)}, u32[32]{0:T(128)}, u32[]{:S(2)}) copy-start(u32[32]{0:T(128)} %constant.31) | copy-start | bytes 388
  4.6 11.3 %copy-start.4 = (f32[288,2]{0,1:T(2,128)S(1)}, f32[288,2]{0,1:T(2,128)}, u32[]{:S(2)}) copy-start(f32[288,2]{0,1:T(2,128)} %param.13) | copy-start | bytes 6916
  5.6 58.6 %all-to-all-start = ((bf16[2,8,1,36,256]{4,0,3,2,1:T(2,128)(2,1)}), bf16[2,8,1,36,256]{4,0,3,2,1:T(2,128)(2,1)S(1)}, u32[]{:S(2)}, u32[]{:S(2)}) async-start(bf16[2,8,1,36,256]{4,0,3,2,1:T(2,128)(2,1)} %copy.17), calls=%async_computation | async-start | bytes 589824 | tf_op jit(solution)/shard_map/all_to_all | solution.py:26
where the time goes:
time: 65.7 us; the launch traced here: 65.4 us
  blocking collectives  44 us (67%)
  starting transfers between devices  7.31 us (11%)
  other arithmetic  5.61 us (9%)
  local copies, waits for them, and re-layouts  3.98 us (6%)
  matrix products  2.36 us (4%)
  between operations  2.15 us (3%)
    unnamed x1, blocking collectives  21.8 us
    psum x1, blocking collectives, shards(): summed = lax.psum(partial_value, 'sp')  17.1 us
    all_to_all x1, starting transfers between devices, shards(): lax.all_to_all(outgoing, 'sp', split_axis=1, concat_axis=2, tiled=True)  7.31 us
    all_gather x1, blocking collectives, shards(): reading = lax.all_gather(own_read, 'tp', axis=0, tiled=True)  5.05 us
    another operation x2, other arithmetic  2.71 us
    reduce_sum x2, other arithmetic, norm_rows(): jnp.mean(wide_rows * wide_rows, axis=-1, keepdims=True) + 1e-06  2.34 us
    unnamed x21, local copies, waits for them, and re-layouts  1.43 us
  transfers between devices with their start and end apart: 1, of which 0 were waited for; matrix products, arithmetic and copies ran while one was open for 9% of the time, Pallas kernels for 0%

commit v1 on v0

--- a/solution.py
+++ b/solution.py
@@ -2,6 +2,7 @@
 import jax.numpy as jnp
 from jax import lax
 from jax.sharding import PartitionSpec as P
+from jax.lax import axis_size, ppermute
 
 HEAD_DIM = 128
 
@@ -45,7 +46,10 @@
     carried = jnp.sum(jnp.where(block_ids > lax.axis_index("sp"), every_total, 0.0), axis=0)
     weights = jnp.exp(jax.nn.log_sigmoid(logits) + inner_sum + carried[None, :])
     partial_value = jnp.einsum("sh,shd->hd", weights, value_heads.astype(jnp.float32))
-    summed = lax.psum(partial_value, "sp")
+    p_count = axis_size("sp")
+    summed = partial_value
+    for k in [[(rr, rr ^ w) for rr in range(p_count)] for w in (1, 2, 4, 8, 16) if w < p_count]:
+        summed = summed + ppermute(summed, "sp", k)
     own_read = summed.reshape(head_width).astype(jnp.bfloat16)
     reading = lax.all_gather(own_read, "tp", axis=0, tiled=True)
     return (key_cache, value_cache, reading)

time: 65.7 us -> 60.3 us (0.918)
  blocking collectives: 44 us -> 26.9 us
  waiting for transfers between devices: 0.01 us -> 11.6 us
    psum x1 -> x0, blocking collectives: 17.1 us -> none  [shards(): summed = lax.psum(partial_value, 'sp')]
    ppermute x0 -> x3, waiting for transfers between devices: none -> 11.6 us  [shards(): summed = summed + ppermute(summed, 'sp', k)]
  transfers between devices with their start and end apart: 1 -> 4, of which waited for: 0 -> 3; matrix products, arithmetic and copies ran while one was open for 9% -> 10% of each run, Pallas kernels for 0% -> 0%
where the time goes in v1:
time: 60.3 us; the launch traced here: 60 us
  blocking collectives  26.9 us (45%)
  waiting for transfers between devices  11.6 us (19%)
  starting transfers between devices  7.32 us (12%)
  other arithmetic  5.62 us (9%)
  local copies, waits for them, and re-layouts  3.98 us (7%)
  matrix products  2.36 us (4%)
  between operations  2.16 us (4%)
    unnamed x1, blocking collectives  21.8 us
    ppermute x3, waiting for transfers between devices, shards(): summed = summed + ppermute(summed, 'sp', k)  11.6 us
    all_to_all x1, starting transfers between devices, shards(): lax.all_to_all(outgoing, 'sp', split_axis=1, concat_axis=2, tiled=True)  7.31 us
    all_gather x1, blocking collectives, shards(): reading = lax.all_gather(own_read, 'tp', axis=0, tiled=True)  5.06 us
    another operation x2, other arithmetic  2.71 us
    reduce_sum x2, other arithmetic, norm_rows(): jnp.mean(wide_rows * wide_rows, axis=-1, keepdims=True) + 1e-06  2.34 us
    unnamed x21, local copies, waits for them, and re-layouts  1.43 us
    dot_general x1, matrix products, shards(): jnp.dot(normed, w_value, preferred_element_type=jnp.float32)  1.3 us
  transfers between devices with their start and end apart: 4, of which 3 were waited for; matrix products, arithmetic and copies ran while one was open for 10% of the time, Pallas kernels for 0%

profile of v1, /device:TPU:0, one launch (start us, length us, event | category | flops | bytes accessed | tf_op | source)
XLA Modules:
  0.0 60.0 jit_solution(8454295339224934806)
XLA Ops:
  0.7 1.7 %fusion = f32[288]{0:T(512)S(1)} fusion(bf16[288,2048]{1,0:T(8,128)(2,1)} %param.7), kind=kLoop, calls=%fused_computation.2 | loop fusion | flops 1769184 | bytes 1180800 | tf_op jit(solution)/shard_map/reduce_sum | solution.py:12
  2.4 0.2 copy-done.1
  2.6 1.3 %convolution_convert_fusion = bf16[288,256]{1,0:T(8,128)(2,1)S(1)} fusion(bf16[2048,256]{1,0:T(8,128)(2,1)S(1)} %copy-done, bf16[288,2048]{1,0:T(8,128)(2,1)S(1)} %copy-done.1, f32[2048]{0:T(1024)} %param.9, f32[288]{0:T(512)S(1)} %add_rsqrt_fusion), kind=kOutput, calls=%fused_computation.5 | convolution fusion | flops 304422912 | bytes 2385024 | tf_op jit(solution)/shard_map/dot_general | solution.py:25
  3.9 0.5 convolution_convert_fusion.1
  4.6 1.0 %copy.17 = bf16[2,8,1,36,256]{4,0,3,2,1:T(2,128)(2,1)} copy(bf16[2,8,1,36,256]{4,3,1,2,0:T(8,128)(2,1)S(1)} %pad_maximum_fusion) | data formatting | bytes 589824 | tf_op jit(solution)/shard_map/stack | solution.py:26
  5.6 7.3 %all-to-all-start = ((bf16[2,8,1,36,256]{4,0,3,2,1:T(2,128)(2,1)}), bf16[2,8,1,36,256]{4,0,3,2,1:T(2,128)(2,1)S(1)}, u32[]{:S(2)}, u32[]{:S(2)}) async-start(bf16[2,8,1,36,256]{4,0,3,2,1:T(2,128)(2,1)} %copy.17), calls=%async_computation | async-start | bytes 589824 | tf_op jit(solution)/shard_map/all_to_all | solution.py:27
  13.0 0.6 %fusion.11 = f32[]{:T(128)} fusion(bf16[2048]{0:T(1024)(128)(2,1)S(1)} %copy-done.3), kind=kLoop, calls=%fused_computation.20 | loop fusion | flops 6143 | bytes 4100 | tf_op jit(solution)/shard_map/reduce_sum | solution.py:12
  14.3 0.2 fusion.21
  14.5 0.1 fusion.8
  14.7 0.6 %dynamic-slice = u32[1]{0:T(128)} dynamic-slice(u32[32]{0:T(128)S(1)} %copy-done.7, u32[]{:T(128)S(6)} %add.60), dynamic_slice_sizes={1} | dynamic-slice | bytes 12
  16.0 0.1 fusion.19
  16.1 0.1 negate_dynamic-update-slice_fusion
  16.2 21.8 %all-reduce.1 = f32[16]{0:T(128)S(1)} all-reduce(f32[16]{0:T(128)S(1)} %negate_dynamic-update-slice_fusion), channel_id=2, replica_groups=mesh['sp'=8,'tp'=4] {'sp'}, use_global_device_ids=true, to_apply=%add.1 | all-reduce | flops 16 | bytes 128
  38.1 2.5 %reduce-window.6 = f32[2,3,128]{2,1,0:T(4,128)S(1)} reduce-window(f32[2,3,128]{2,1,0:T(4,128)S(1)} %reshape.81, f32[]{:T(128)} %constant.20.clone.1), window={size=1x1x128 pad=0_0x0_0x0_127}, to_apply=%region_2.3 | reduce-window | flops 97536 | bytes 6148 | tf_op jit(solution)/shard_map/reduce-window
  40.6 0.1 slice_reduce_fusion
  40.7 0.2 reduce-window.9
  41.3 0.1 fusion.5
  41.4 3.6 %collective-permute-done = f32[2,128]{1,0:T(2,128)S(1)} collective-permute-done((f32[2,128]{1,0:T(2,128)S(1)}, f32[2,128]{1,0:T(2,128)S(1)}, u32[]{:S(2)}, u32[]{:S(2)}) %collective-permute-start) | collective-permute-done | bytes 1056 | tf_op jit(solution)/shard_map/ppermute | solution.py:52
  45.0 3.6 %collective-permute-done.1 = f32[2,128]{1,0:T(2,128)S(1)} collective-permute-done((f32[2,128]{1,0:T(2,128)S(1)}, f32[2,128]{1,0:T(2,128)S(1)}, u32[]{:S(2)}, u32[]{:S(2)}) %collective-permute-start.1) | collective-permute-done | bytes 1056 | tf_op jit(solution)/shard_map/ppermute | solution.py:52
  48.6 4.5 %collective-permute-done.2 = f32[2,128]{1,0:T(2,128)S(1)} collective-permute-done((f32[2,128]{1,0:T(2,128)S(1)}, f32[2,128]{1,0:T(2,128)S(1)}, u32[]{:S(2)}, u32[]{:S(2)}) %collective-permute-start.2) | collective-permute-done | bytes 1056 | tf_op jit(solution)/shard_map/ppermute | solution.py:52
  53.1 5.1 %all-gather.1 = bf16[4,1,256]{2,1,0:T(2,128)(2,1)S(1)} all-gather(bf16[1,1,256]{2,1,0:T(2,128)(2,1)S(1)} %reshape.88), channel_id=1, replica_groups=mesh['sp'=8,'tp'=4] {'tp'}, dimensions={0}, use_global_device_ids=true | all-gather | bytes 2560 | tf_op jit(solution)/shard_map/all_gather | solution.py:54
  58.2 0.6 copy.31
  58.7 0.4 fusion.20
  59.2 0.8 %copy_bitcast_fusion = (bf16[1,8,36,256]{3,1,2,0:T(8,128)(2,1)}, bf16[1,8,36,256]{3,1,2,0:T(8,128)(2,1)}) fusion(bf16[1,8,1,36,256]{4,0,3,2,1:T(2,128)(2,1)S(1)} %get-tuple-element.11, bf16[1,8,1,36,256]{4,0,3,2,1:T(2,128)(2,1)S(1)} %get-tuple-element.12), kind=kLoop, calls=%fused_computation.14 | loop fusion | bytes 589824 | tf_op jit(solution)/shard_map/squeeze | solution.py:29
  (42 shorter events, 0.7 us)
Async XLA Ops:
  0.6 1.8 %copy-start = (bf16[2048,256]{1,0:T(8,128)(2,1)S(1)}, bf16[2048,256]{1,0:T(8,128)(2,1)}, u32[]{:S(2)}) copy-start(bf16[2048,256]{1,0:T(8,128)(2,1)} %param.11) | copy-start | bytes 3145732
  0.6 1.9 %copy-start.1 = (bf16[288,2048]{1,0:T(8,128)(2,1)S(1)}, bf16[288,2048]{1,0:T(8,128)(2,1)}, u32[]{:S(2)}) copy-start(bf16[288,2048]{1,0:T(8,128)(2,1)} %param.7) | copy-start | bytes 3538948
  2.6 1.3 %copy-start.5 = (f32[2048]{0:T(1024)S(1)}, f32[2048]{0:T(1024)}, u32[]{:S(2)}) copy-start(f32[2048]{0:T(1024)} %param.9) | copy-start | bytes 24580
  2.6 1.3 %copy-start.6 = (bf16[2048,256]{1,0:T(8,128)(2,1)S(1)}, bf16[2048,256]{1,0:T(8,128)(2,1)}, u32[]{:S(2)}) copy-start(bf16[2048,256]{1,0:T(8,128)(2,1)} %param.10) | copy-start | bytes 3145732
  4.5 8.5 %copy-start.3 = (bf16[2048]{0:T(1024)(128)(2,1)S(1)}, bf16[2048]{0:T(1024)(128)(2,1)}, u32[]{:S(2)}) copy-start(bf16[2048]{0:T(1024)(128)(2,1)} %param.8) | copy-start | bytes 12292
  4.5 9.8 %copy-start.2 = (bf16[2048,256]{1,0:T(8,128)(2,1)S(1)}, bf16[2048,256]{1,0:T(8,128)(2,1)}, u32[]{:S(2)}) copy-start(bf16[2048,256]{1,0:T(8,128)(2,1)} %param.12) | copy-start | bytes 3145732
  4.6 10.1 %copy-start.7 = (u32[32]{0:T(128)S(1)}, u32[32]{0:T(128)}, u32[]{:S(2)}) copy-start(u32[32]{0:T(128)} %constant.31) | copy-start | bytes 388
  4.6 11.3 %copy-start.4 = (f32[288,2]{0,1:T(2,128)S(1)}, f32[288,2]{0,1:T(2,128)}, u32[]{:S(2)}) copy-start(f32[288,2]{0,1:T(2,128)} %param.13) | copy-start | bytes 6916
  5.6 53.1 %all-to-all-start = ((bf16[2,8,1,36,256]{4,0,3,2,1:T(2,128)(2,1)}), bf16[2,8,1,36,256]{4,0,3,2,1:T(2,128)(2,1)S(1)}, u32[]{:S(2)}, u32[]{:S(2)}) async-start(bf16[2,8,1,36,256]{4,0,3,2,1:T(2,128)(2,1)} %copy.17), calls=%async_computation | async-start | bytes 589824 | tf_op jit(solution)/shard_map/all_to_all | solution.py:27
  41.4 3.6 %collective-permute-start = (f32[2,128]{1,0:T(2,128)S(1)}, f32[2,128]{1,0:T(2,128)S(1)}, u32[]{:S(2)}, u32[]{:S(2)}) collective-permute-start(f32[2,128]{1,0:T(2,128)S(1)} %bitcast.64), channel_id=1, source_target_pairs={{0,4},{4,0},{8,12},{12,8},{16,20},{20,16},{24,28},{28,24},{1,5},{5... | collective-permute-start | bytes 3080 | tf_op jit(solution)/shard_map/ppermute | solution.py:52
  45.0 3.6 %collective-permute-start.1 = (f32[2,128]{1,0:T(2,128)S(1)}, f32[2,128]{1,0:T(2,128)S(1)}, u32[]{:S(2)}, u32[]{:S(2)}) collective-permute-start(f32[2,128]{1,0:T(2,128)S(1)} %add.57), channel_id=1, source_target_pairs={{0,8},{4,12},{8,0},{12,4},{16,24},{20,28},{24,16},{28,20},{1,9},{5... | collective-permute-start | bytes 3080 | tf_op jit(solution)/shard_map/ppermute | solution.py:52
  48.6 4.5 %collective-permute-start.2 = (f32[2,128]{1,0:T(2,128)S(1)}, f32[2,128]{1,0:T(2,128)S(1)}, u32[]{:S(2)}, u32[]{:S(2)}) collective-permute-start(f32[2,128]{1,0:T(2,128)S(1)} %add.58), channel_id=1, source_target_pairs={{0,16},{4,20},{8,24},{12,28},{16,0},{20,4},{24,8},{28,12},{1,17},{... | collective-permute-start | bytes 3080 | tf_op jit(solution)/shard_map/ppermute | solution.py:52
